TPU v7x, 32 devices: a whole 2x2x4 slice. The times are simulated.
32 devices in a mesh: ep: 8 (over z, core), tp: 4 (over y, x).
Axes of the slice: x: 2, y: 2, z: 4, core: 2. Of those that a mesh axis runs over, the one named last changes fastest.
Arguments:
- tokens: bfloat16 [1536, 4096], P('ep'), may hold values from -6 to 6
- expert_ids: int32 [1536, 2], P('ep'), may hold values from 0 to 7, all different within a row; in each aligned block of 192 rows (0 to 191, 192 to 383, ...) at most 60 rows name the same one
- route_weight: float32 [1536, 2], P('ep'), may hold values from 0.1 to 1
- norm_gain: float32 [4096], replicated, may hold values from 0.1 to 1.9
- gate_weight: bfloat16 [8, 4096, 4096], P('ep', None, 'tp'), may hold values from -0.28125 to 0.28125
- up_weight: bfloat16 [8, 4096, 4096], P('ep', None, 'tp'), may hold values from -0.28125 to 0.28125
- down_weight: bfloat16 [8, 4096, 4096], P('ep', None, 'tp'), may hold values from -0.028076172 to 0.028076172
Outputs:
- mixed: bfloat16 [1536, 4096], P('ep', 'tp')
Inputs may be any that keep to these rules, and one draw needn't show every extreme that they name: `expert_ids`: each row names 2 different experts. In each aligned block of 192 rows (the tokens of one index of ep) no expert is named by more than 60 rows, and in some block some expert is named by exactly 60 rows.
All inputs are finite; a program needn't handle non-finite values.
Results may differ from a plain program's by a relative error of at most 0.007.
Values may be sent and summed in bfloat16 or wider, within the bound.
A program may use at most 64 MiB of HBM per device.

v0:
```python
import jax
import jax.numpy as jnp
from jax import lax
from jax.sharding import PartitionSpec as P

EPS = 1e-06
LIMIT = 7.0
ALPHA = 1.702


def rms_norm(tokens, norm_gain):
    values = tokens.astype(jnp.float32)
    scale = lax.rsqrt(jnp.mean(values * values, axis=-1, keepdims=True) + EPS)
    return (values * scale * norm_gain).astype(jnp.bfloat16)


def clamped_unit(gate_pre, up_pre):
    gate = jnp.minimum(gate_pre, LIMIT)
    up_part = jnp.clip(up_pre, -LIMIT, LIMIT)
    return ((up_part + 1.0) * gate * jax.nn.sigmoid(ALPHA * gate)).astype(jnp.bfloat16)


def slot_numbers(id_blocks, experts, capacity):
    onehot = (id_blocks[:, :, None] == jnp.arange(experts, dtype=jnp.int32)[None, None, :]).astype(
        jnp.int32
    )
    before = jnp.cumsum(onehot, axis=1) - onehot
    position = jnp.sum(before * onehot, axis=2)
    return id_blocks * capacity + position


def project_down(hidden, down_weight):
    result = jnp.einsum(
        "sejf,efd->sejd",
        lax.all_gather(hidden, "tp", axis=3, tiled=True),
        down_weight,
        preferred_element_type=jnp.float32,
    )
    return result.astype(jnp.bfloat16)


def on_device(tokens, expert_ids, route_weight, norm_gain, gate_weight, up_weight, down_weight):
    n_ep = lax.axis_size("ep")
    n_tp = lax.axis_size("tp")
    tok_rows, width = tokens.shape
    top = expert_ids.shape[1]
    local_experts = gate_weight.shape[0]
    experts = local_experts * n_ep
    capacity = 5 * tok_rows * top // (4 * experts)
    cols = width // n_tp
    normed = rms_norm(tokens, norm_gain)
    dest = slot_numbers(expert_ids.reshape(1, tok_rows * top), experts, capacity).reshape(-1)
    slot_range = jnp.arange(experts * capacity, dtype=jnp.int32)
    match = slot_range[:, None] == dest[None, :]
    pick = jnp.any(match.reshape(experts * capacity, tok_rows, top), axis=2).astype(jnp.bfloat16)
    own = lax.dynamic_slice_in_dim(normed, lax.axis_index("tp") * cols, cols, 1)
    buffer = jnp.dot(pick, own, preferred_element_type=jnp.float32).astype(jnp.bfloat16)
    buffer = buffer.reshape(n_ep, local_experts, capacity, cols)
    arrived = lax.all_to_all(buffer, "ep", split_axis=0, concat_axis=0, tiled=True)
    piece = lax.all_gather(arrived, "tp", axis=3, tiled=True)
    gate_part = jnp.einsum("sejd,edf->sejf", piece, gate_weight, preferred_element_type=jnp.float32)
    up_part = jnp.einsum("sejd,edf->sejf", piece, up_weight, preferred_element_type=jnp.float32)
    hidden = clamped_unit(gate_part, up_part)
    result = project_down(hidden, down_weight)
    back = lax.all_to_all(result, "ep", split_axis=0, concat_axis=0, tiled=True).reshape(
        experts * capacity, cols
    )
    chosen = jnp.transpose(match).astype(jnp.bfloat16)
    per_copy = jnp.dot(chosen, back, preferred_element_type=jnp.float32).reshape(
        tok_rows, top, cols
    )
    mixed = jnp.sum(per_copy * route_weight[:, :, None], axis=1)
    return mixed.astype(jnp.bfloat16)


def solution(mesh):
    placed = (
        P("ep", None),
        P("ep", None),
        P("ep", None),
        P(),
        P("ep", None, "tp"),
        P("ep", None, "tp"),
        P("ep", None, "tp"),
    )
    return jax.shard_map(
        on_device, mesh=mesh, in_specs=placed, out_specs=P("ep", "tp"), check_vma=False
    )
```

profile of v0, /device:TPU:0, one launch (start us, length us, event | category | flops | bytes accessed | tf_op | source)
XLA Modules:
  0.0 220.5 jit_solution(3522461065963199480)
XLA Ops:
  6.5 0.0 copy-start
  6.5 0.0 all-gather.3.cloned.1.call-start
  6.5 0.0 copy-start.1
  6.5 3.5 %convert_element_type.41 = f32[192,4096]{1,0:T(8,128)} convert(bf16[192,4096]{1,0:T(8,128)(2,1)} %param.7) | non-fusion elementwise | flops 786432 | bytes 4718592 | tf_op jit(solution)/shard_map/convert_element_type | solution.py:12
  10.1 0.0 copy-done
  10.1 0.4 multiply_reduce_fusion
  10.5 0.0 copy-done.1
  10.5 0.1 copy.28
  10.6 0.1 reshape.211
  10.8 0.9 reduce-window.6
  11.6 0.2 slice_reduce_fusion
  11.9 0.1 fusion.36
  12.0 0.1 reduce_sum.30
  12.1 0.1 copy.29
  12.2 0.2 fusion.30
  12.4 0.7 dynamic-slice
  13.1 1.6 convolution_convert_fusion
  14.8 0.2 reshape.217
  14.9 32.8 %all_to_all.10 = bf16[8,1,60,1024]{3,2,1,0:T(8,128)(2,1)} all-to-all(bf16[8,1,60,1024]{3,2,1,0:T(8,128)(2,1)S(1)} %bitcast.73), channel_id=1, replica_groups=mesh['ep'=8,'tp'=4] {'ep'}, dimensions={0} | all-to-all | bytes 1966080 | tf_op jit(solution)/shard_map/all_to_all | solution.py:59
  47.8 0.0 all-gather.3.cloned.1.call-update
  47.8 0.0 all-gather.5.cloned.1.call-start
  47.8 51.6 %all-gather.3.cloned.1.call-done = bf16[8,1,60,4096]{3,2,0,1:T(8,128)(2,1)} async-done(((bf16[8,1,60,1024]{3,2,0,1:T(8,128)(2,1)}), bf16[8,1,60,4096]{3,2,0,1:T(8,128)(2,1)}) %all-gather.3.cloned.1.call-update) | async-done | bytes 3932176 | tf_op jit(solution)/shard_map/all_gather | solution.py:60
  99.4 0.0 copy-start.2
  99.4 9.1 %fusion.2 = f32[8,60,1024]{2,1,0:T(8,128)S(1)} fusion(bf16[1,4096,1024]{2,1,0:T(8,128)(2,1)} %param.11, bf16[8,1,60,4096]{3,2,0,1:T(8,128)(2,1)} %all-gather.3.cloned.1.call-done), kind=kOutput, calls=%fused_computation.2 | convolution fusion | flops 4026531840 | bytes 14286848 | tf_op jit(solution)/shard_map/sejd,edf->sejf/dot_general | solution.py:61
  108.6 0.0 copy-done.2
  108.6 9.4 %fusion.23 = bf16[8,1,60,1024]{3,2,0,1:T(8,128)(2,1)} fusion(f32[8,60,1024]{2,1,0:T(8,128)S(1)} %fusion.2, bf16[1,4096,1024]{2,1,0:T(8,128)(2,1)} %param.12, bf16[8,1,60,4096]{3,2,0,1:T(8,128)(2,1)S(1)} %copy-done.2), kind=kOutput, calls=%fused_computation.15 | convolution fusion | flops 4031447040 | bytes 15269888 | tf_op jit(solution)/shard_map/sejd,edf->sejf/dot_general | solution.py:62
  118.0 0.0 all-gather.5.cloned.1.call-update
  118.0 52.7 %all-gather.5.cloned.1.call-done = bf16[8,1,60,4096]{3,2,0,1:T(8,128)(2,1)} async-done(((bf16[8,1,60,1024]{3,2,0,1:T(8,128)(2,1)}), bf16[8,1,60,4096]{3,2,0,1:T(8,128)(2,1)}) %all-gather.5.cloned.1.call-update) | async-done | bytes 3932176 | tf_op jit(solution)/shard_map/all_gather | solution.py:35
  170.7 10.1 %fusion.18 = bf16[8,1,60,1024]{3,2,1,0:T(8,128)(2,1)} fusion(bf16[1,4096,1024]{2,1,0:T(8,128)(2,1)} %param.13, bf16[8,1,60,4096]{3,2,0,1:T(8,128)(2,1)} %all-gather.5.cloned.1.call-done), kind=kOutput, calls=%fused_computation.14 | convolution fusion | flops 4027023360 | bytes 13303808 | tf_op jit(solution)/shard_map/sejf,efd->sejd/dot_general | solution.py:33
  180.8 0.0 copy-start.3
  180.8 4.7 %all-to-all-start.1 = ((bf16[8,1,60,1024]{3,2,1,0:T(8,128)(2,1)}), bf16[8,1,60,1024]{3,2,1,0:T(8,128)(2,1)S(1)}, u32[]{:S(2)}, u32[]{:S(2)}) async-start(bf16[8,1,60,1024]{3,2,1,0:T(8,128)(2,1)} %fusion.18), calls=%async_computation.1 | async-start | bytes 2097152 | tf_op jit(solution)/shard_map/all_to_all | solution.py:65
  185.6 0.2 iota_compare_fusion.1
  185.8 0.3 eq.60
  186.0 26.1 %all-to-all-done.1 = bf16[8,1,60,1024]{3,2,1,0:T(8,128)(2,1)S(1)} async-done(((bf16[8,1,60,1024]{3,2,1,0:T(8,128)(2,1)}), bf16[8,1,60,1024]{3,2,1,0:T(8,128)(2,1)S(1)}, u32[]{:S(2)}, u32[]{:S(2)}) %all-to-all-start.1) | async-done | bytes 983072 | tf_op jit(solution)/shard_map/all_to_all | solution.py:65
  212.1 0.2 reshape.235
  212.3 0.0 copy-done.3
  212.3 1.4 multiply_reduce_fusion.1
  (8 shorter events, 0.0 us)
Async XLA Ops:
  6.5 3.6 %copy-start = (bf16[192,4096]{1,0:T(8,128)(2,1)S(1)}, bf16[192,4096]{1,0:T(8,128)(2,1)}, u32[]{:S(2)}) copy-start(bf16[192,4096]{1,0:T(8,128)(2,1)} %param.7) | copy-start | bytes 4718596
  6.5 92.9 %all-gather.3.cloned.1.call-start = ((), (), s32[]{:S(2)}) async-start(), calls=%async_computation.2 | async-start | bytes 5242880 | tf_op jit(solution)/shard_map/all_gather | solution.py:60
  6.5 4.0 %copy-start.1 = (s32[192,2]{0,1:T(2,128)S(1)}, s32[192,2]{0,1:T(2,128)}, u32[]{:S(2)}) copy-start(s32[192,2]{0,1:T(2,128)} %param.8) | copy-start | bytes 4612
  47.8 122.9 %all-gather.5.cloned.1.call-start = ((), (), s32[]{:S(2)}) async-start(), calls=%async_computation.3 | async-start | bytes 5242880 | tf_op jit(solution)/shard_map/all_gather | solution.py:35
  99.4 9.1 %copy-start.2 = (bf16[8,1,60,4096]{3,2,0,1:T(8,128)(2,1)S(1)}, bf16[8,1,60,4096]{3,2,0,1:T(8,128)(2,1)}, u32[]{:S(2)}) copy-start(bf16[8,1,60,4096]{3,2,0,1:T(8,128)(2,1)} %all-gather.3.cloned.1.call-done) | copy-start | bytes 11796484
  180.8 31.5 %copy-start.3 = (f32[192,2]{0,1:T(2,128)S(1)}, f32[192,2]{0,1:T(2,128)}, u32[]{:S(2)}) copy-start(f32[192,2]{0,1:T(2,128)} %param.9) | copy-start | bytes 4612
  180.8 31.3 %all-to-all-start.1 = ((bf16[8,1,60,1024]{3,2,1,0:T(8,128)(2,1)}), bf16[8,1,60,1024]{3,2,1,0:T(8,128)(2,1)S(1)}, u32[]{:S(2)}, u32[]{:S(2)}) async-start(bf16[8,1,60,1024]{3,2,1,0:T(8,128)(2,1)} %fusion.18), calls=%async_computation.1 | async-start | bytes 2097152 | tf_op jit(solution)/shard_map/all_to_all | solution.py:65
Sparse Core Ops, SparseCore 0:
  47.9 51.4 all-gather.2
  118.1 52.5 all-gather.4
where the time goes:
time: 221 us
  waiting for transfers between devices  130 us (59%)
  blocking collectives  32.8 us (15%)
  matrix products  31.6 us (14%)
  between operations  13.5 us (6%)
  other arithmetic  5.26 us (2%)
  starting transfers between devices  4.78 us (2%)
    all_gather x1, waiting for transfers between devices, project_down(): lax.all_gather(hidden, 'tp', axis=3, tiled=True)  52.7 us
    all_gather x1, waiting for transfers between devices, on_device(): piece = lax.all_gather(arrived, 'tp', axis=3, tiled=True)  51.6 us
    all_to_all x1, blocking collectives, on_device(): lax.all_to_all(buffer, 'ep', split_axis=0, concat_axis=0, tiled=True)  32.8 us
    all_to_all x1, waiting for transfers between devices, on_device(): lax.all_to_all(result, 'ep', split_axis=0, concat_axis=0, tiled=True)  26.1 us
    dot_general x1, matrix products, project_down(): jnp.einsum('sejf,efd->sejd', lax.all_gather(hidden, 'tp', axis=3, tiled=T...  10.1 us
    dot_general x1, matrix products, on_device(): jnp.einsum('sejd,edf->sejf', piece, up_weight, preferred_element_type=jnp...  9.37 us
    dot_general x1, matrix products, on_device(): jnp.einsum('sejd,edf->sejf', piece, gate_weight, preferred_element_type=j...  9.13 us
    all_to_all x1, starting transfers between devices, on_device(): lax.all_to_all(result, 'ep', split_axis=0, concat_axis=0, tiled=True)  4.74 us
  transfers between devices with their start and end apart: 3, of which 3 were waited for; matrix products, arithmetic and copies ran while one was open for 0% of the time, Pallas kernels for 0%

commit v1 on v0

--- a/solution.py
+++ b/solution.py
@@ -30,12 +30,37 @@
 
 
 def project_down(hidden, down_weight):
+    raw_out, x_now, z2 = (jax.lax.axis_size("tp"), jax.lax.axis_index("tp"), hidden.shape[3])
+    blocks_here = [(num, (num + 1) % raw_out) for num in range(raw_out)]
+    store = [(num, (num - 1) % raw_out) for num in range(raw_out)]
+    inter = raw_out // 2
+    e_now = a_next = hidden
     result = jnp.einsum(
         "sejf,efd->sejd",
-        lax.all_gather(hidden, "tp", axis=3, tiled=True),
-        down_weight,
+        hidden,
+        lax.dynamic_slice_in_dim(down_weight, x_now * z2, hidden.shape[3], axis=1),
         preferred_element_type=jnp.float32,
     )
+    for pp in range(1, inter + 1):
+        e_now = jax.lax.ppermute(e_now, "tp", blocks_here)
+        if pp < raw_out - inter:
+            a_next = jax.lax.ppermute(a_next, "tp", perm=store)
+            result = result + jnp.einsum(
+                "sejf,efd->sejd",
+                a_next,
+                lax.dynamic_slice_in_dim(
+                    down_weight, (x_now + pp) % raw_out * z2, a_next.shape[3], axis=1
+                ),
+                preferred_element_type=jnp.float32,
+            )
+        result = result + jnp.einsum(
+            "sejf,efd->sejd",
+            e_now,
+            lax.dynamic_slice_in_dim(
+                down_weight, (x_now - pp) % raw_out * z2, e_now.shape[3], axis=1
+            ),
+            preferred_element_type=jnp.float32,
+        )
     return result.astype(jnp.bfloat16)
 
 

time: 221 us -> 226 us (1.023)
  starting transfers between devices: 4.78 us -> 8.29 us
    ppermute x0 -> x3, waiting for transfers between devices: none -> 54.1 us  [the longest x2 39.7 us: project_down(): e_now = jax.lax.ppermute(e_now, 'tp', blocks_here)]
    all_gather x1 -> x0, waiting for transfers between devices: 52.7 us -> none  [project_down(): lax.all_gather(hidden, 'tp', axis=3, tiled=True)]
    ppermute x0 -> x3, starting transfers between devices: none -> 3.55 us  [the longest x2 2.09 us: project_down(): e_now = jax.lax.ppermute(e_now, 'tp', blocks_here)]
    dot_general x1 -> x4, matrix products: 10.1 us -> 11.1 us  [the longest x2 5.52 us: project_down(): jnp.einsum('sejf,efd->sejd', e_now, lax.dynamic_slice_in_dim(down_weight,...]
  transfers between devices with their start and end apart: 3 -> 5, of which waited for: 3 -> 5; matrix products, arithmetic and copies ran while one was open for 0% -> 4% of each run, Pallas kernels for 0% -> 0%
where the time goes in v1:
time: 226 us; the launch traced here: 225 us
  waiting for transfers between devices  132 us (58%)
  blocking collectives  32.8 us (15%)
  matrix products  31.4 us (14%)
  between operations  13.6 us (6%)
  starting transfers between devices  8.29 us (4%)
  local copies, waits for them, and re-layouts  3.75 us (2%)
  other arithmetic  3.58 us (2%)
    all_gather x1, waiting for transfers between devices, on_device(): piece = lax.all_gather(arrived, 'tp', axis=3, tiled=True)  51.7 us
    ppermute x2, waiting for transfers between devices, project_down(): e_now = jax.lax.ppermute(e_now, 'tp', blocks_here)  39.7 us
    all_to_all x1, blocking collectives, on_device(): lax.all_to_all(buffer, 'ep', split_axis=0, concat_axis=0, tiled=True)  32.8 us
    all_to_all x1, waiting for transfers between devices, on_device(): lax.all_to_all(result, 'ep', split_axis=0, concat_axis=0, tiled=True)  26.1 us
    ppermute x1, waiting for transfers between devices, project_down(): a_next = jax.lax.ppermute(a_next, 'tp', perm=store)  14.5 us
    dot_general x1, matrix products, on_device(): jnp.einsum('sejd,edf->sejf', piece, gate_weight, preferred_element_type=j...  9.13 us
    dot_general x1, matrix products, on_device(): jnp.einsum('sejd,edf->sejf', piece, up_weight, preferred_element_type=jnp...  8.38 us
    dot_general x2, matrix products, project_down(): jnp.einsum('sejf,efd->sejd', e_now, lax.dynamic_slice_in_dim(down_weight,...  5.52 us
  transfers between devices with their start and end apart: 5, of which 5 were waited for; matrix products, arithmetic and copies ran while one was open for 4% of the time, Pallas kernels for 0%

profile of v1, /device:TPU:0, one launch (start us, length us, event | category | flops | bytes accessed | tf_op | source)
XLA Modules:
  0.0 225.4 jit_solution(4510957676317232278)
XLA Ops:
  6.5 0.0 all-gather.2.cloned.1.call-start
  6.5 0.0 copy-start
  6.5 0.0 copy-start.1
  6.5 1.9 convert_element_type.33
  8.4 0.0 copy-done
  8.4 0.4 multiply_reduce_fusion
  8.8 0.0 copy-done.1
  8.8 0.1 copy.38
  9.0 0.1 reshape.235
  9.1 0.9 reduce-window.6
  10.0 0.2 slice_reduce_fusion
  10.2 0.1 fusion.41
  10.3 0.1 reduce_sum.30
  10.5 0.1 copy.39
  10.6 0.2 fusion.35
  10.7 0.7 dynamic-slice
  11.4 1.5 convolution_convert_fusion
  12.9 1.3 reshape.242
  14.3 32.8 %all_to_all.10 = bf16[8,1,60,1024]{3,2,1,0:T(8,128)(2,1)} all-to-all(bf16[8,1,60,1024]{3,2,1,0:T(8,128)(2,1)S(1)} %bitcast.81), channel_id=1, replica_groups=mesh['ep'=8,'tp'=4] {'ep'}, dimensions={0} | all-to-all | bytes 1966080 | tf_op jit(solution)/shard_map/all_to_all | solution.py:84
  47.1 0.0 all-gather.2.cloned.1.call-update
  47.1 51.7 %all-gather.2.cloned.1.call-done = bf16[8,1,60,4096]{3,2,0,1:T(8,128)(2,1)} async-done(((bf16[8,1,60,1024]{3,2,0,1:T(8,128)(2,1)}), bf16[8,1,60,4096]{3,2,0,1:T(8,128)(2,1)}) %all-gather.2.cloned.1.call-update) | async-done | bytes 3932176 | tf_op jit(solution)/shard_map/all_gather | solution.py:85
  98.8 0.0 copy-start.2
  98.8 9.1 %fusion = f32[8,60,1024]{2,1,0:T(8,128)S(1)} fusion(bf16[1,4096,1024]{2,1,0:T(8,128)(2,1)} %param.11, bf16[8,1,60,4096]{3,2,0,1:T(8,128)(2,1)} %all-gather.2.cloned.1.call-done), kind=kOutput, calls=%fused_computation | convolution fusion | flops 4026531840 | bytes 14286848 | tf_op jit(solution)/shard_map/sejd,edf->sejf/dot_general | solution.py:86
  107.9 0.0 copy-done.2
  107.9 8.4 %multiply_convert_fusion = bf16[8,60,1024]{2,1,0:T(8,128)(2,1)S(1)} fusion(f32[8,60,1024]{2,1,0:T(8,128)S(1)} %fusion, bf16[1,4096,1024]{2,1,0:T(8,128)(2,1)} %param.12, bf16[8,1,60,4096]{3,2,0,1:T(8,128)(2,1)S(1)} %copy-done.2), kind=kOutput, calls=%fused_computation.15 | convolution fusion | flops 4031447040 | bytes 15269888 | tf_op jit(solution)/shard_map/sejd,edf->sejf/dot_general | solution.py:87
  116.3 0.5 copy.42
  116.9 1.5 collective-permute-start.1
  118.4 1.5 collective-permute-start
  119.8 22.6 %collective-permute-done.1 = bf16[8,1,60,1024]{3,0,2,1:T(8,128)(2,1)S(1)} collective-permute-done((bf16[8,1,60,1024]{3,0,2,1:T(8,128)(2,1)S(1)}, bf16[8,1,60,1024]{3,0,2,1:T(8,128)(2,1)S(1)}, u32[]{:S(2)}, u32[]{:S(2)}) %collective-permute-start.1) | collective-permute-done | bytes 983072 | tf_op jit(solution)/shard_map/ppermute | solution.py:45
  142.4 0.6 collective-permute-start.2
  143.0 0.0 slice-start
  143.0 3.0 %fusion.12 = f32[1024,8,60]{0,2,1:T(8,128)S(1)} fusion(bf16[8,60,1024]{2,1,0:T(8,128)(2,1)S(1)} %multiply_convert_fusion, bf16[1,4096,1024]{2,1,0:T(8,128)(2,1)} %param.13, s32[]{:T(128)S(6)} %select_n.28), kind=kOutput, calls=%fused_computation.13 | convolution fusion | flops 1006632960 | bytes 5046276 | tf_op jit(solution)/shard_map/sejf,efd->sejd/dot_general | solution.py:38
  146.0 0.0 slice-start.1
  146.0 3.1 %fusion.8 = f32[1024,8,60]{0,2,1:T(8,128)S(1)} fusion(bf16[1,4096,1024]{2,1,0:T(8,128)(2,1)} %param.13, s32[]{:T(128)S(6)} %select_n.32, bf16[8,1,60,1024]{3,0,2,1:T(8,128)(2,1)S(1)} %collective-permute-done.1), kind=kOutput, calls=%fused_computation.9 | convolution fusion | flops 1006632960 | bytes 5046276 | tf_op jit(solution)/shard_map/sejf,efd->sejd/dot_general | solution.py:56
  149.1 14.5 %collective-permute-done = bf16[8,1,60,1024]{3,0,2,1:T(8,128)(2,1)} collective-permute-done((bf16[8,1,60,1024]{3,0,2,1:T(8,128)(2,1)S(1)}, bf16[8,1,60,1024]{3,0,2,1:T(8,128)(2,1)}, u32[]{:S(2)}, u32[]{:S(2)}) %collective-permute-start) | collective-permute-done | bytes 983072 | tf_op jit(solution)/shard_map/ppermute | solution.py:47
  163.6 0.0 slice-done
  163.6 0.0 slice-done.1
  163.6 2.6 %fusion.10 = f32[1024,8,60]{0,2,1:T(8,128)S(1)} fusion(bf16[1,4096,1024]{2,1,0:T(8,128)(2,1)S(1)} %bitcast.85, s32[]{:T(128)S(6)} %select_n.30, bf16[8,1,60,1024]{3,0,2,1:T(8,128)(2,1)} %collective-permute-done), kind=kOutput, calls=%fused_computation.11 | convolution fusion | flops 1006632960 | bytes 5046276 | tf_op jit(solution)/shard_map/sejf,efd->sejd/dot_general | solution.py:48
  166.2 17.1 %collective-permute-done.2 = bf16[8,1,60,1024]{3,0,2,1:T(8,128)(2,1)S(1)} collective-permute-done((bf16[8,1,60,1024]{3,0,2,1:T(8,128)(2,1)S(1)}, bf16[8,1,60,1024]{3,0,2,1:T(8,128)(2,1)S(1)}, u32[]{:S(2)}, u32[]{:S(2)}) %collective-permute-start.2) | collective-permute-done | bytes 983072 | tf_op jit(solution)/shard_map/ppermute | solution.py:45
  183.3 2.4 %fusion.24 = bf16[8,1,60,1024]{3,2,1,0:T(8,128)(2,1)} fusion(bf16[1,4096,1024]{2,1,0:T(8,128)(2,1)S(1)} %bitcast.85, s32[]{:T(128)S(6)} %select_n.34, f32[1024,8,60]{0,2,1:T(8,128)S(1)} %fusion.8, f32[1024,8,60]{0,2,1:T(8,128)S(1)} %fusion.12, f32[1024,8,60]{0,2,1:T(8,128)S(1)} %fusion.10, bf16[8,1,60,1024]{3,0,2,1:T(8,128)(2,1)S(1)} %collective-permute-done.2), kind=kOutput, calls=%fused_computation.23 | convolution fusion | flops 1008599040 | bytes 10354692 | tf_op jit(solution)/shard_map/sejf,efd->sejd/dot_general | solution.py:56
  185.7 0.0 copy-start.3
  185.7 4.7 %all-to-all-start.1 = ((bf16[8,1,60,1024]{3,2,1,0:T(8,128)(2,1)}), bf16[8,1,60,1024]{3,2,1,0:T(8,128)(2,1)S(1)}, u32[]{:S(2)}, u32[]{:S(2)}) async-start(bf16[8,1,60,1024]{3,2,1,0:T(8,128)(2,1)} %fusion.24), calls=%async_computation.1 | async-start | bytes 2097152 | tf_op jit(solution)/shard_map/all_to_all | solution.py:90
  190.4 0.2 iota_compare_fusion.1
  190.6 0.3 eq.64
  190.9 26.1 %all-to-all-done.1 = bf16[8,1,60,1024]{3,2,1,0:T(8,128)(2,1)S(1)} async-done(((bf16[8,1,60,1024]{3,2,1,0:T(8,128)(2,1)}), bf16[8,1,60,1024]{3,2,1,0:T(8,128)(2,1)S(1)}, u32[]{:S(2)}, u32[]{:S(2)}) %all-to-all-start.1) | async-done | bytes 983072 | tf_op jit(solution)/shard_map/all_to_all | solution.py:90
  217.0 0.2 reshape.268
  217.2 0.0 copy-done.3
  217.2 1.4 multiply_reduce_fusion.1
  (9 shorter events, 0.0 us)
Async XLA Ops:
  6.5 92.2 %all-gather.2.cloned.1.call-start = ((), (), s32[]{:S(2)}) async-start(), calls=%async_computation.2 | async-start | bytes 5242880 | tf_op jit(solution)/shard_map/all_gather | solution.py:85
  6.5 1.9 copy-start
  6.5 2.3 %copy-start.1 = (s32[192,2]{0,1:T(2,128)S(1)}, s32[192,2]{0,1:T(2,128)}, u32[]{:S(2)}) copy-start(s32[192,2]{0,1:T(2,128)} %param.8) | copy-start | bytes 4612
  98.8 9.1 %copy-start.2 = (bf16[8,1,60,4096]{3,2,0,1:T(8,128)(2,1)S(1)}, bf16[8,1,60,4096]{3,2,0,1:T(8,128)(2,1)}, u32[]{:S(2)}) copy-start(bf16[8,1,60,4096]{3,2,0,1:T(8,128)(2,1)} %all-gather.2.cloned.1.call-done) | copy-start | bytes 11796484
  116.9 25.6 %collective-permute-start.1 = (bf16[8,1,60,1024]{3,0,2,1:T(8,128)(2,1)S(1)}, bf16[8,1,60,1024]{3,0,2,1:T(8,128)(2,1)S(1)}, u32[]{:S(2)}, u32[]{:S(2)}) collective-permute-start(bf16[8,1,60,1024]{3,0,2,1:T(8,128)(2,1)S(1)} %copy.42), channel_id=1, source_target_pairs={{0,1},{1,2},{2,3},{3,0},{4,5},{5,6},{6,7},{7,4},{8,9},{9,10},{10,1... | collective-permute-start | bytes 2949128 | tf_op jit(solution)/shard_map/ppermute | solution.py:45
  118.4 45.2 %collective-permute-start = (bf16[8,1,60,1024]{3,0,2,1:T(8,128)(2,1)S(1)}, bf16[8,1,60,1024]{3,0,2,1:T(8,128)(2,1)}, u32[]{:S(2)}, u32[]{:S(2)}) collective-permute-start(bf16[8,1,60,1024]{3,0,2,1:T(8,128)(2,1)S(1)} %copy.42), channel_id=1, source_target_pairs={{0,3},{1,0},{2,1},{3,2},{4,7},{5,4},{6,5},{7,6},{8,11},{9,8},{10,9... | collective-permute-start | bytes 2949128 | tf_op jit(solution)/shard_map/ppermute | solution.py:47
  142.4 40.8 %collective-permute-start.2 = (bf16[8,1,60,1024]{3,0,2,1:T(8,128)(2,1)S(1)}, bf16[8,1,60,1024]{3,0,2,1:T(8,128)(2,1)S(1)}, u32[]{:S(2)}, u32[]{:S(2)}) collective-permute-start(bf16[8,1,60,1024]{3,0,2,1:T(8,128)(2,1)S(1)} %collective-permute-done.1), channel_id=1, source_target_pairs={{0,1},{1,2},{2,3},{3,0},{4,5},{5,6},{6,7},{7,4},{8,9},{9,10},{10,1... | collective-permute-start | bytes 2949128 | tf_op jit(solution)/shard_map/ppermute | solution.py:45
  143.0 20.6 %slice-start = ((s8[8388608]{0:T(1024)(128)(4,1)}), s8[4194304]{0:T(1024)(128)(4,1)S(1)}, s32[]{:S(2)}) async-start(s8[8388608]{0:T(1024)(128)(4,1)} %bitcast.84), calls=%async_computation.3 | async-start | bytes 8388608
  146.0 17.6 %slice-start.1 = ((s8[8388608]{0:T(1024)(128)(4,1)}), s8[4194304]{0:T(1024)(128)(4,1)S(1)}, s32[]{:S(2)}) async-start(s8[8388608]{0:T(1024)(128)(4,1)} %bitcast.84), calls=%async_computation.4 | async-start | bytes 8388608
  185.7 31.5 %copy-start.3 = (f32[192,2]{0,1:T(2,128)S(1)}, f32[192,2]{0,1:T(2,128)}, u32[]{:S(2)}) copy-start(f32[192,2]{0,1:T(2,128)} %param.9) | copy-start | bytes 4612
  185.7 31.3 %all-to-all-start.1 = ((bf16[8,1,60,1024]{3,2,1,0:T(8,128)(2,1)}), bf16[8,1,60,1024]{3,2,1,0:T(8,128)(2,1)S(1)}, u32[]{:S(2)}, u32[]{:S(2)}) async-start(bf16[8,1,60,1024]{3,2,1,0:T(8,128)(2,1)} %fusion.24), calls=%async_computation.1 | async-start | bytes 2097152 | tf_op jit(solution)/shard_map/all_to_all | solution.py:90
Sparse Core Ops, SparseCore 0:
  47.2 51.4 all-gather.1
